TPU v7x, 32 devices: a whole 2x2x4 slice. The times are simulated.
32 devices in a mesh: sp: 8 (over z, x), tp: 4 (over y, core).
Axes of the slice: x: 2, y: 2, z: 4, core: 2. Of those that a mesh axis runs over, the one named last changes fastest.
Arguments:
- tokens: bfloat16 [8, 80, 4096], P(None, 'sp', 'tp'), may hold values from -6 to 6
- latent_down_weight: bfloat16 [4096, 512], replicated, may hold values from -0.09375 to 0.09375
- w_rope_key: bfloat16 [4096, 64], replicated, may hold values from -0.09375 to 0.09375
- latent_norm_gain: float32 [512], replicated, may hold values from 0.1 to 1.9
- key_up_weight: bfloat16 [512, 4096], P(None, 'tp'), may hold values from -0.25 to 0.25
- value_up_weight: bfloat16 [512, 4096], P(None, 'tp'), may hold values from -0.25 to 0.25
- cached_latent_rows: bfloat16 [8, 32768, 512], P('sp', 'tp'), may hold values from -6 to 6
- past_rope: bfloat16 [8, 32768, 64], P('sp', 'tp'), may hold values from -6 to 6
- query_nope: bfloat16 [8, 4096], P('sp', 'tp'), may hold values from -8 to 8
- query_rope: bfloat16 [8, 2048], P('sp', 'tp'), may hold values from -300 to 300
Outputs:
- new_keys: bfloat16 [8, 80, 4096], P('sp', None, 'tp')
- new_values: bfloat16 [8, 80, 4096], P('sp', None, 'tp')
- new_rope: bfloat16 [8, 80, 64], P('sp')
- attended: bfloat16 [8, 4096], P('sp', 'tp')
All inputs are finite; a program needn't handle non-finite values.
Results may differ from a plain program's by a relative error of at most 0.0085.
Values may be sent and summed in bfloat16 or wider, within the bound.
A program may use at most 64 MiB of HBM per device.

v0:
```python
import jax
import jax.numpy as jnp
from jax import lax
from jax.sharding import PartitionSpec as P

PLAIN_KEY_WIDTH = 128
ROPE = 64
VALUE_WIDTH = 128
PAST_POSITIONS = 32768
epsilon = 1e-06
rope_theta = 10000.0


def combined_all(part, axis, combine):
    gathered = jax.tree.map(lambda a: lax.all_gather(a, axis), part)

    def take(source):
        return jax.tree.map(lambda a: lax.dynamic_index_in_dim(a, source, 0, False), gathered)

    return lax.fori_loop(
        1, lax.axis_size(axis), lambda source, state: combine(state, take(source)), take(0)
    )


def rotate(values, positions):
    halfway = values.shape[-1] // 2
    frequency = rope_theta ** (-jnp.arange(halfway, dtype=jnp.float32) / halfway)
    angles = positions[:, None] * frequency
    first = values[..., :halfway]
    second = values[..., halfway:]
    return jnp.concatenate(
        [
            first * jnp.cos(angles) - second * jnp.sin(angles),
            first * jnp.sin(angles) + second * jnp.cos(angles),
        ],
        axis=-1,
    )


def combine_parts(first, second):
    highest = jnp.maximum(first[0], second[0])
    scale_first = jnp.exp(first[0] - highest)
    scale_second = jnp.exp(second[0] - highest)
    total = first[1] * scale_first + second[1] * scale_second
    summed = first[2] * scale_first[..., None] + second[2] * scale_second[..., None]
    return (highest, total, summed)


def on_device(
    tokens,
    latent_down_weight,
    w_rope_key,
    latent_norm_gain,
    key_up_weight,
    value_up_weight,
    cached_latent_rows,
    past_rope,
    query_nope,
    query_rope,
):
    rows_here = lax.all_to_all(tokens, "sp", split_axis=0, concat_axis=1, tiled=True)
    prompts, per_seq, features = rows_here.shape
    row_count = prompts * per_seq
    latent_width = latent_down_weight.shape[1]
    turn_width = w_rope_key.shape[1]
    factor = (PLAIN_KEY_WIDTH + ROPE) ** (-0.5)
    fragment = lax.all_gather(rows_here, "tp", axis=2, tiled=True)
    columns = fragment.shape[2]
    flat_rows = fragment.reshape(row_count, columns)
    latent_raw = jnp.dot(flat_rows, latent_down_weight, preferred_element_type=jnp.float32)
    rope_raw = jnp.dot(flat_rows, w_rope_key, preferred_element_type=jnp.float32)
    scale = lax.rsqrt(jnp.mean(latent_raw * latent_raw, axis=-1, keepdims=True) + epsilon)
    latent = (latent_raw * scale * latent_norm_gain).astype(jnp.bfloat16)
    positions = (PAST_POSITIONS + jnp.arange(per_seq)).astype(jnp.float32)
    rope_local = rotate(rope_raw.reshape(prompts, per_seq, turn_width), positions).astype(
        jnp.bfloat16
    )
    keys_local = (
        jnp.dot(latent, key_up_weight, preferred_element_type=jnp.float32)
        .astype(jnp.bfloat16)
        .reshape(prompts, per_seq, key_up_weight.shape[1])
    )
    values_local = (
        jnp.dot(latent, value_up_weight, preferred_element_type=jnp.float32)
        .astype(jnp.bfloat16)
        .reshape(prompts, per_seq, value_up_weight.shape[1])
    )
    new_keys, new_values, new_rope = (keys_local, values_local, rope_local)
    owned = query_nope.shape[0]
    heads_local = query_nope.shape[1] // PLAIN_KEY_WIDTH
    query_own = query_nope.reshape(owned, heads_local, PLAIN_KEY_WIDTH)
    turn_own = query_rope.reshape(owned, heads_local, ROPE)
    head_keys = key_up_weight.reshape(latent_width, heads_local, PLAIN_KEY_WIDTH)
    query_latent = jnp.einsum(
        "shd,khd->shk", query_own, head_keys, preferred_element_type=jnp.float32
    ).astype(jnp.bfloat16)
    every_latent, every_turn = (
        lax.all_gather(query_latent, "tp", axis=1, tiled=True),
        lax.all_gather(turn_own, "tp", axis=1, tiled=True),
    )
    past_scores = jnp.einsum(
        "shk,spk->shp", every_latent, cached_latent_rows, preferred_element_type=jnp.float32
    )
    past_scores = (
        past_scores
        + jnp.einsum("shd,spd->shp", every_turn, past_rope, preferred_element_type=jnp.float32)
    ) * factor
    local_peak = jnp.max(past_scores, axis=-1)
    local_weight = jnp.exp(past_scores - local_peak[:, :, None])
    local_total = jnp.sum(local_weight, axis=-1)
    local_latent = jnp.einsum(
        "shp,spk->shk",
        local_weight.astype(jnp.bfloat16),
        cached_latent_rows,
        preferred_element_type=jnp.float32,
    )
    peak_all, total_all, latent_all = combined_all(
        (local_peak, local_total, local_latent), "tp", combine_parts
    )
    start = lax.axis_index("tp") * heads_local
    past_peak = lax.dynamic_slice_in_dim(peak_all, start, heads_local, 1)
    past_total = lax.dynamic_slice_in_dim(total_all, start, heads_local, 1)
    past_sum = lax.dynamic_slice_in_dim(latent_all, start, heads_local, 1)
    fresh = new_keys.shape[1]
    new_scores = jnp.einsum(
        "shd,sphd->shp",
        query_own,
        new_keys.reshape(owned, fresh, heads_local, PLAIN_KEY_WIDTH),
        preferred_element_type=jnp.float32,
    )
    new_scores = (
        new_scores
        + jnp.einsum("shd,spd->shp", turn_own, new_rope, preferred_element_type=jnp.float32)
    ) * factor
    peak = jnp.maximum(past_peak, jnp.max(new_scores, axis=-1))
    past_share = jnp.exp(past_peak - peak)
    new_weight = jnp.exp(new_scores - peak[:, :, None])
    denominator = past_total * past_share + jnp.sum(new_weight, axis=-1)
    latent_sum = (past_sum * past_share[..., None]).astype(jnp.bfloat16)
    head_values = value_up_weight.reshape(latent_width, heads_local, VALUE_WIDTH)
    past_out = jnp.einsum(
        "shk,khd->shd", latent_sum, head_values, preferred_element_type=jnp.float32
    )
    new_out = jnp.einsum(
        "shp,sphd->shd",
        new_weight.astype(jnp.bfloat16),
        new_values.reshape(owned, fresh, heads_local, VALUE_WIDTH),
        preferred_element_type=jnp.float32,
    )
    attended = (
        ((past_out + new_out) / denominator[:, :, None])
        .astype(jnp.bfloat16)
        .reshape(owned, heads_local * VALUE_WIDTH)
    )
    return (new_keys, new_values, new_rope, attended)


def solution(mesh):
    in_specs = (
        P(None, "sp", "tp"),
        P(),
        P(),
        P(),
        P(None, "tp"),
        P(None, "tp"),
        P("sp", "tp", None),
        P("sp", "tp", None),
        P("sp", "tp"),
        P("sp", "tp"),
    )
    out_specs = (P("sp", None, "tp"), P("sp", None, "tp"), P("sp", None, None), P("sp", "tp"))
    return jax.shard_map(
        on_device, mesh=mesh, in_specs=in_specs, out_specs=out_specs, check_vma=False
    )
```

profile of v0, /device:TPU:0, one launch (start us, length us, event | category | flops | bytes accessed | tf_op | source)
XLA Modules:
  0.0 66.8 jit_solution(9695988542635753334)
XLA Ops:
  0.6 0.0 copy-start
  0.6 1.8 %copy.21 = bf16[8,10,1024]{2,1,0:T(8,128)(2,1)} copy(bf16[8,10,1024]{2,0,1:T(8,128)(2,1)} %param.12) | data formatting | bytes 327680 | tf_op args[0]
  2.4 7.3 %all-to-all-start = ((bf16[8,10,1024]{2,1,0:T(8,128)(2,1)}), bf16[8,10,1024]{2,1,0:T(8,128)(2,1)}, u32[]{:S(2)}, u32[]{:S(2)}) async-start(bf16[8,10,1024]{2,1,0:T(8,128)(2,1)} %copy.21), calls=%async_computation | async-start | bytes 524288 | tf_op jit(solution)/shard_map/all_to_all | solution.py:61
  9.7 0.7 %reduce.8 = bf16[512]{0:T(512)(128)(2,1)S(1)} reduce(bf16[1,512]{1,0:T(2,128)(2,1)} %param.21, bf16[]{:T(256)} %constant.97), dimensions={0}, to_apply=%param.21.reduce_sub_computation | reduce | bytes 2050 | tf_op args[9]
  10.4 0.1 reshape.326
  10.5 5.2 %all_gather.29 = bf16[1,32,64]{2,1,0:T(8,128)(2,1)S(1)} all-gather(bf16[1,8,64]{2,1,0:T(8,128)(2,1)S(1)} %reshape.326), channel_id=1, replica_groups=mesh['sp'=8,'tp'=4] {'tp'}, dimensions={1}, use_global_device_ids=true | all-gather | bytes 5120 | tf_op jit(solution)/shard_map/all_gather | solution.py:99
  15.7 1.6 %fusion.18 = bf16[8,1,512]{2,1,0:T(2,128)(2,1)S(1)} fusion(bf16[1,1024]{1,0:T(2,128)(2,1)} %param.20, bf16[512,1024]{1,0:T(8,128)(2,1)} %param.16), kind=kOutput, calls=%fused_computation.28 | convolution fusion | flops 1048576 | bytes 1058816 | tf_op jit(solution)/shard_map/shd,khd->shk/dot_general | solution.py:94
  17.3 5.2 %all-gather = bf16[32,512]{1,0:T(8,128)(2,1)S(1)} all-gather(bf16[8,512]{1,0:T(8,128)(2,1)S(1)} %bitcast.161), channel_id=2, replica_groups=mesh['sp'=8,'tp'=4] {'tp'}, dimensions={0}, use_global_device_ids=true | all-gather | bytes 40960 | tf_op jit(solution)/shard_map/all_gather | solution.py:98
  22.5 0.0 copy-start.7
  22.5 5.9 %fusion.11 = f32[32,8192]{1,0:T(8,128)S(1)} fusion(bf16[32,512]{1,0:T(8,128)(2,1)S(1)} %all-gather, bf16[1,8192,512]{2,1,0:T(8,128)(2,1)} %param.18), kind=kOutput, calls=%fused_computation.17 | convolution fusion | flops 268435456 | bytes 9469952 | tf_op jit(solution)/shard_map/shk,spk->shp/dot_general | solution.py:101
  28.4 0.0 copy-done
  28.4 0.4 fusion.64
  28.8 0.4 fusion.23
  29.2 0.0 copy-done.7
  29.2 0.6 dynamic-slice
  30.5 0.2 dynamic-update-slice
  30.7 0.2 dynamic-update-slice.1
  30.9 7.1 %all-reduce.2 = (f32[128]{0:T(128)S(1)}, f32[128]{0:T(128)S(1)}) all-reduce(f32[128]{0:T(128)S(1)} %dynamic-update-slice, f32[128]{0:T(128)S(1)} %dynamic-update-slice.1), channel_id=3, replica_groups=mesh['sp'=8,'tp'=4] {'tp'}, use_global_device_ids=true, to_apply=%add | all-reduce | flops 256 | bytes 2048
  38.0 0.1 reshape.336
  38.1 0.1 reshape.337
  38.2 0.0 copy-start.1
  38.2 0.0 copy-start.5
  38.2 5.1 %fusion.9 = f32[32,512]{1,0:T(8,128)S(1)} fusion(bf16[1,8192,512]{2,1,0:T(8,128)(2,1)} %param.18, f32[32,8192]{1,0:T(8,128)S(1)} %get-tuple-element.237, f32[32]{0:T(128)S(1)} %get-tuple-element.236), kind=kOutput, calls=%fused_computation.15 | convolution fusion | flops 268959744 | bytes 9502848 | tf_op jit(solution)/shard_map/shp,spk->shk/dot_general | solution.py:111
  43.2 0.0 copy-start.6
  43.2 0.0 copy-start.2
  43.2 5.9 %all-gather.3 = f32[128,512]{1,0:T(8,128)S(1)} all-gather(f32[32,512]{1,0:T(8,128)S(1)} %fusion.9), channel_id=5, replica_groups=mesh['sp'=8,'tp'=4] {'tp'}, dimensions={0}, use_global_device_ids=true | all-gather | bytes 327680 | tf_op jit(solution)/shard_map/all_gather | solution.py:15
  49.2 0.5 while.19
  49.2 0.1 fusion.80
  49.4 0.1 fusion.80
  49.5 0.1 fusion.80
  49.6 0.1 reshape.330
  49.7 0.0 all-to-all-done
  49.7 1.0 %all_to_all.10 = bf16[1,80,1024]{2,1,0:T(8,128)(2,1)S(1)} reshape(bf16[8,10,1024]{2,1,0:T(8,128)(2,1)} %all-to-all-done) | data formatting | bytes 327680 | tf_op jit(solution)/shard_map/all_to_all | solution.py:61
  50.7 8.0 %all_gather.27 = bf16[1,80,4096]{2,1,0:T(8,128)(2,1)S(1)} all-gather(bf16[1,80,1024]{2,1,0:T(8,128)(2,1)S(1)} %all_to_all.10), channel_id=1, replica_groups=mesh['sp'=8,'tp'=4] {'tp'}, dimensions={2}, use_global_device_ids=true | all-gather | bytes 819200 | tf_op jit(solution)/shard_map/all_gather | solution.py:67
  58.7 3.1 %multiply_reduce_fusion = (f32[80]{0:T(128)S(1)}, f32[80,512]{1,0:T(8,128)S(1)}) fusion(bf16[4096,512]{1,0:T(8,128)(2,1)} %param.13, bf16[1,80,4096]{2,1,0:T(8,128)(2,1)S(1)} %all_gather.27), kind=kOutput, calls=%fused_computation.46 | convolution fusion | flops 335626176 | bytes 5013824 | tf_op jit(solution)/shard_map/dot_general | solution.py:70
  61.9 0.0 copy-done.1
  61.9 0.0 copy-done.5
  61.9 0.4 convolution_convert_fusion.1
  62.3 0.0 copy-done.6
  62.3 0.0 copy-start.3
  62.3 0.2 fusion.32
  62.5 1.4 %convolution_bitcast_fusion = f32[1,80,64]{1,2,0:T(8,128)S(1)} fusion(bf16[4096,64]{0,1:T(8,128)(2,1)} %param.14, bf16[1,80,4096]{2,1,0:T(8,128)(2,1)S(1)} %all_gather.27), kind=kOutput, calls=%fused_computation.21 | convolution fusion | flops 41943040 | bytes 1200128 | tf_op jit(solution)/shard_map/dot_general | solution.py:71
  63.9 0.0 copy-done.2
  63.9 0.4 convolution_convert_fusion
  64.3 0.0 copy-start.4
  64.3 0.1 fusion.40
  64.4 0.6 pad_maximum_fusion
  65.0 0.2 fusion.63
  65.3 0.1 fusion.59
  65.3 0.2 fusion.54
  65.5 0.1 fusion.61
  65.6 0.1 fusion.47
  65.7 0.3 fusion.15
  66.0 0.2 fusion.29
  66.1 0.1 fusion.55
  66.2 0.6 copy.64
  66.8 0.0 copy-done.3
  66.8 0.0 copy-done.4
  (17 shorter events, 0.1 us)
Async XLA Ops:
  0.6 27.8 %copy-start = (bf16[1,8192,64]{1,2,0:T(8,128)(2,1)S(1)}, bf16[1,8192,64]{1,2,0:T(8,128)(2,1)}, u32[]{:S(2)}) copy-start(bf16[1,8192,64]{1,2,0:T(8,128)(2,1)} %param.19) | copy-start | bytes 3145732
  2.4 47.3 %all-to-all-start = ((bf16[8,10,1024]{2,1,0:T(8,128)(2,1)}), bf16[8,10,1024]{2,1,0:T(8,128)(2,1)}, u32[]{:S(2)}, u32[]{:S(2)}) async-start(bf16[8,10,1024]{2,1,0:T(8,128)(2,1)} %copy.21), calls=%async_computation | async-start | bytes 524288 | tf_op jit(solution)/shard_map/all_to_all | solution.py:61
  22.5 6.7 %copy-start.7 = (u32[32]{0:T(128)S(1)}, u32[32]{0:T(128)}, u32[]{:S(2)}) copy-start(u32[32]{0:T(128)} %constant.87) | copy-start | bytes 388
  38.2 23.7 %copy-start.1 = (bf16[512,1024]{1,0:T(8,128)(2,1)S(1)}, bf16[512,1024]{1,0:T(8,128)(2,1)}, u32[]{:S(2)}) copy-start(bf16[512,1024]{1,0:T(8,128)(2,1)} %param.16) | copy-start | bytes 3145732
  38.2 23.7 %copy-start.5 = (f32[512]{0:T(512)S(1)}, f32[512]{0:T(512)}, u32[]{:S(2)}) copy-start(f32[512]{0:T(512)} %param.15) | copy-start | bytes 6148
  43.2 19.0 %copy-start.6 = (bf16[1,1024]{1,0:T(2,128)(2,1)S(1)}, bf16[1,1024]{1,0:T(2,128)(2,1)}, u32[]{:S(2)}) copy-start(bf16[1,1024]{1,0:T(2,128)(2,1)} %param.20) | copy-start | bytes 6148
  43.2 20.7 %copy-start.2 = (bf16[512,1024]{1,0:T(8,128)(2,1)S(1)}, bf16[512,1024]{1,0:T(8,128)(2,1)}, u32[]{:S(2)}) copy-start(bf16[512,1024]{1,0:T(8,128)(2,1)} %param.17) | copy-start | bytes 3145732
  62.3 4.5 %copy-start.3 = (bf16[80,1024]{1,0:T(8,128)(2,1)}, bf16[80,1024]{1,0:T(8,128)(2,1)S(1)}, u32[]{:S(2)}) copy-start(bf16[80,1024]{1,0:T(8,128)(2,1)S(1)} %convolution_convert_fusion.1) | copy-start | bytes 491524
  64.3 2.6 %copy-start.4 = (bf16[80,1024]{1,0:T(8,128)(2,1)}, bf16[80,1024]{1,0:T(8,128)(2,1)S(1)}, u32[]{:S(2)}) copy-start(bf16[80,1024]{1,0:T(8,128)(2,1)S(1)} %convolution_convert_fusion) | copy-start | bytes 491524
where the time goes:
time: 67.3 us; the launch traced here: 66.8 us
  blocking collectives  31.4 us (47%)
  matrix products  19.1 us (28%)
  starting transfers between devices  7.28 us (11%)
  local copies, waits for them, and re-layouts  4.87 us (7%)
  other arithmetic  2.69 us (4%)
  between operations  1.45 us (2%)
    all_gather x1, blocking collectives, on_device(): fragment = lax.all_gather(rows_here, 'tp', axis=2, tiled=True)  7.99 us
    all_to_all x1, starting transfers between devices, on_device(): lax.all_to_all(tokens, 'sp', split_axis=0, concat_axis=1, tiled=True)  7.28 us
    unnamed x1, blocking collectives  7.09 us
    dot_general x1, matrix products, on_device(): jnp.einsum('shk,spk->shp', every_latent, cached_latent_rows, preferred_el...  5.92 us
    all_gather x1, blocking collectives, combined_all(): gathered = jax.tree.map(lambda a: lax.all_gather(a, axis), part)  5.91 us
    all_gather x1, blocking collectives, on_device(): lax.all_gather(query_latent, 'tp', axis=1, tiled=True)  5.19 us
    all_gather x1, blocking collectives, on_device(): lax.all_gather(turn_own, 'tp', axis=1, tiled=True)  5.18 us
    dot_general x1, matrix products, on_device(): jnp.einsum('shp,spk->shk', local_weight.astype(jnp.bfloat16), cached_late...  5.06 us
  transfers between devices with their start and end apart: 1, of which 0 were waited for; matrix products, arithmetic and copies ran while one was open for 24% of the time, Pallas kernels for 0%

commit v1 on v0

--- a/solution.py
+++ b/solution.py
@@ -9,6 +9,19 @@
 PAST_POSITIONS = 32768
 epsilon = 1e-06
 rope_theta = 10000.0
+
+
+def scan_the_tables(sheet, axis_no, raw):
+    placed, y_new = (sheet.shape[:axis_no], sheet.shape[axis_no + 1 :])
+    tmp = jnp.moveaxis(sheet.reshape(*placed, raw, -1, *y_new), axis_no, 0)
+    return tmp
+
+
+def lift_windows(load, at_axis):
+    t1 = list(load.shape[1:])
+    t1[at_axis] *= load.shape[0]
+    q_next = jnp.moveaxis(load, 0, at_axis).reshape(t1)
+    return q_next
 
 
 def combined_all(part, axis, combine):
@@ -58,7 +71,14 @@
     query_nope,
     query_rope,
 ):
-    rows_here = lax.all_to_all(tokens, "sp", split_axis=0, concat_axis=1, tiled=True)
+    o_now, step_out = (lax.psum(1, "sp"), lax.axis_index("sp"))
+    r_now = scan_the_tables(tokens, 0, o_now)
+    so_far_all = [r_now[step_out]]
+    for u in tuple(range(1, o_now)):
+        long_array = r_now[step_out ^ u]
+        so_far_all.append(lax.ppermute(long_array, "sp", [(j, j ^ u) for j in range(o_now)]))
+    r_now = jnp.stack(so_far_all)[step_out ^ jnp.arange(o_now)]
+    rows_here = lift_windows(r_now, 1)
     prompts, per_seq, features = rows_here.shape
     row_count = prompts * per_seq
     latent_width = latent_down_weight.shape[1]

time: 67.3 us -> 95.6 us (1.42)
  local copies, waits for them, and re-layouts: 4.87 us -> 23.6 us
  other arithmetic: 2.69 us -> 10.1 us
  starting transfers between devices: 7.28 us -> 12.7 us
  matrix products: 19.1 us -> 15.9 us
    ppermute x0 -> x7, starting transfers between devices: none -> 12.7 us  [on_device(): lax.ppermute(long_array, 'sp', [(j, j ^ u) for j in range(o_now)])]
    unnamed x23 -> x52, local copies, waits for them, and re-layouts: 3.5 us -> 13.5 us
    all_to_all x1 -> x0, starting transfers between devices: 7.28 us -> none  [on_device(): lax.all_to_all(tokens, 'sp', split_axis=0, concat_axis=1, tiled=True)]
    exp x3, other arithmetic: 0.07 us -> 3.78 us  [combine_parts(): scale_second = jnp.exp(second[0] - highest)]
    dot_general x1, matrix products: 5.06 us -> 1.62 us  [on_device(): jnp.einsum('shp,spk->shk', local_weight.astype(jnp.bfloat16), cached_late...]
    another operation x1 -> x3, local copies, waits for them, and re-layouts: 0.08 us -> 2.66 us
    squeeze x0 -> x1, local copies, waits for them, and re-layouts: none -> 2.24 us  [on_device(): long_array = r_now[step_out ^ u]]
    mul x3, other arithmetic: 0.03 us -> 2 us  [combine_parts(): first[2] * scale_first[..., None] + second[2] * scale_second[..., None]]
  transfers between devices with their start and end apart: 1 -> 7, of which waited for: 0 -> 1; matrix products, arithmetic and copies ran while one was open for 24% -> 37% of each run, Pallas kernels for 0% -> 0%
where the time goes in v1:
time: 95.6 us; the launch traced here: 94.9 us
  blocking collectives  30.6 us (32%)
  local copies, waits for them, and re-layouts  23.6 us (25%)
  matrix products  15.9 us (17%)
  starting transfers between devices  12.7 us (13%)
  other arithmetic  10.1 us (11%)
  between operations  1.66 us (2%)
    unnamed x52, local copies, waits for them, and re-layouts  13.5 us
    ppermute x7, starting transfers between devices, on_device(): lax.ppermute(long_array, 'sp', [(j, j ^ u) for j in range(o_now)])  12.7 us
    all_gather x1, blocking collectives, on_device(): fragment = lax.all_gather(rows_here, 'tp', axis=2, tiled=True)  7.41 us
    unnamed x1, blocking collectives  7.09 us
    dot_general x1, matrix products, on_device(): jnp.einsum('shk,spk->shp', every_latent, cached_latent_rows, preferred_el...  6.05 us
    all_gather x1, blocking collectives, combined_all(): gathered = jax.tree.map(lambda a: lax.all_gather(a, axis), part)  5.76 us
    all_gather x1, blocking collectives, on_device(): lax.all_gather(query_latent, 'tp', axis=1, tiled=True)  5.19 us
    all_gather x1, blocking collectives, on_device(): lax.all_gather(turn_own, 'tp', axis=1, tiled=True)  5.18 us
  transfers between devices with their start and end apart: 7, of which 1 were waited for; matrix products, arithmetic and copies ran while one was open for 37% of the time, Pallas kernels for 0%

profile of v1, /device:TPU:0, one launch (start us, length us, event | category | flops | bytes accessed | tf_op | source)
XLA Modules:
  0.0 94.9 jit_solution(10290553117644959446)
XLA Ops:
  0.7 2.2 %constant_dynamic-slice_fusion.4 = (bf16[1,10,1024]{2,0,1:T(2,128)(2,1)S(1)}, bf16[1,10,1024]{2,0,1:T(2,128)(2,1)S(1)}, bf16[1,10,1024]{2,0,1:T(2,128)(2,1)S(1)}...) fusion(bf16[8,10,1024]{2,0,1:T(8,128)(2,1)} %param.12, ...), kind=kLoop, calls=%fused_computation.89 | loop fusion | bytes 327712 | tf_op jit(solution)/shard_map/squeeze | solution.py:78
  2.9 0.6 copy.46
  3.6 3.0 %collective-permute-start = (bf16[1,10,1024]{2,1,0:T(8,128)(2,1)}, bf16[1,10,1024]{2,1,0:T(8,128)(2,1)}, u32[]{:S(2)}, u32[]{:S(2)}) collective-permute-start(bf16[1,10,1024]{2,1,0:T(8,128)(2,1)} %copy.46), channel_id=1, source_target_pairs={{0,4},{4,0},{8,12},{12,8},{16,20},{20,16},{24,28},{28,24},{1,5},{5... | collective-permute-start | bytes 61448 | tf_op jit(solution)/shard_map/ppermute | solution.py:79
  6.5 0.6 copy.47
  7.1 1.6 %collective-permute-start.1 = (bf16[1,10,1024]{2,1,0:T(8,128)(2,1)}, bf16[1,10,1024]{2,1,0:T(8,128)(2,1)}, u32[]{:S(2)}, u32[]{:S(2)}) collective-permute-start(bf16[1,10,1024]{2,1,0:T(8,128)(2,1)} %copy.47), channel_id=1, source_target_pairs={{0,8},{4,12},{8,0},{12,4},{16,24},{20,28},{24,16},{28,20},{1,9},{5... | collective-permute-start | bytes 61448 | tf_op jit(solution)/shard_map/ppermute | solution.py:79
  8.7 0.6 copy.48
  9.3 0.6 copy.49
  10.0 3.0 %collective-permute-start.3 = (bf16[1,10,1024]{2,1,0:T(8,128)(2,1)}, bf16[1,10,1024]{2,1,0:T(8,128)(2,1)}, u32[]{:S(2)}, u32[]{:S(2)}) collective-permute-start(bf16[1,10,1024]{2,1,0:T(8,128)(2,1)} %copy.49), channel_id=1, source_target_pairs={{0,16},{4,20},{8,24},{12,28},{16,0},{20,4},{24,8},{28,12},{1,17},{... | collective-permute-start | bytes 61448 | tf_op jit(solution)/shard_map/ppermute | solution.py:79
  13.0 0.6 copy.50
  13.6 1.3 %collective-permute-start.4 = (bf16[1,10,1024]{2,1,0:T(8,128)(2,1)}, bf16[1,10,1024]{2,1,0:T(8,128)(2,1)}, u32[]{:S(2)}, u32[]{:S(2)}) collective-permute-start(bf16[1,10,1024]{2,1,0:T(8,128)(2,1)} %copy.50), channel_id=1, source_target_pairs={{0,20},{4,16},{8,28},{12,24},{16,4},{20,0},{24,12},{28,8},{1,21},{... | collective-permute-start | bytes 61448 | tf_op jit(solution)/shard_map/ppermute | solution.py:79
  14.9 0.6 add_convert_fusion
  15.4 0.7 reduce.8
  16.2 0.6 copy-done.7
  16.8 5.2 %all_gather.29 = bf16[1,32,64]{2,1,0:T(8,128)(2,1)S(1)} all-gather(bf16[1,8,64]{2,1,0:T(8,128)(2,1)S(1)} %reshape.355), channel_id=1, replica_groups=mesh['sp'=8,'tp'=4] {'tp'}, dimensions={1}, use_global_device_ids=true | all-gather | bytes 5120 | tf_op jit(solution)/shard_map/all_gather | solution.py:119
  22.0 1.8 %fusion.18 = bf16[8,1,512]{2,1,0:T(2,128)(2,1)S(1)} fusion(bf16[1,1024]{1,0:T(2,128)(2,1)} %param.20, bf16[512,1024]{1,0:T(8,128)(2,1)} %param.16), kind=kOutput, calls=%fused_computation.29 | convolution fusion | flops 1048576 | bytes 1058816 | tf_op jit(solution)/shard_map/shd,khd->shk/dot_general | solution.py:114
  23.7 5.2 %all-gather = bf16[32,512]{1,0:T(8,128)(2,1)S(1)} all-gather(bf16[8,512]{1,0:T(8,128)(2,1)S(1)} %bitcast.185), channel_id=2, replica_groups=mesh['sp'=8,'tp'=4] {'tp'}, dimensions={0}, use_global_device_ids=true | all-gather | bytes 40960 | tf_op jit(solution)/shard_map/all_gather | solution.py:118
  28.9 6.1 %fusion.11 = f32[32,8192]{1,0:T(8,128)S(1)} fusion(bf16[32,512]{1,0:T(8,128)(2,1)S(1)} %all-gather, bf16[1,8192,512]{2,1,0:T(8,128)(2,1)} %param.18), kind=kOutput, calls=%fused_computation.18 | convolution fusion | flops 268435456 | bytes 9469952 | tf_op jit(solution)/shard_map/shk,spk->shp/dot_general | solution.py:121
  35.0 0.4 fusion.66
  35.4 0.4 fusion.23
  35.8 1.6 %fusion.9 = f32[32,512]{1,0:T(8,128)S(1)} fusion(bf16[1,8192,512]{2,1,0:T(8,128)(2,1)S(1)} %bitcast.180, f32[32,8192]{1,0:T(8,128)S(1)} %get-tuple-element.238, f32[32]{0:T(128)S(1)} %get-tuple-element.237), kind=kOutput, calls=%fused_computation.16 | convolution fusion | flops 268959744 | bytes 9502848 | tf_op jit(solution)/shard_map/shp,spk->shk/dot_general | solution.py:131
  37.5 0.6 dynamic-slice.11
  38.7 0.2 dynamic-update-slice
  39.0 0.2 dynamic-update-slice.1
  39.2 7.1 %all-reduce.2 = (f32[128]{0:T(128)S(1)}, f32[128]{0:T(128)S(1)}) all-reduce(f32[128]{0:T(128)S(1)} %dynamic-update-slice, f32[128]{0:T(128)S(1)} %dynamic-update-slice.1), channel_id=3, replica_groups=mesh['sp'=8,'tp'=4] {'tp'}, use_global_device_ids=true, to_apply=%add | all-reduce | flops 256 | bytes 2048
  46.3 0.7 reshape.375
  46.9 0.6 slice_bitcast_fusion.1
  47.5 0.7 reshape.376
  48.2 0.6 pad_clamp_fusion
  48.8 0.6 fusion.35
  49.4 5.8 %all-gather.3 = f32[128,512]{1,0:T(8,128)S(1)} all-gather(f32[32,512]{1,0:T(8,128)S(1)} %fusion.9), channel_id=5, replica_groups=mesh['sp'=8,'tp'=4] {'tp'}, dimensions={0}, use_global_device_ids=true | all-gather | bytes 327680 | tf_op jit(solution)/shard_map/all_gather | solution.py:28
  55.2 7.6 %while.19 = (s32[]{:T(128)}, f32[1,32]{1,0:T(1,128)}, f32[1,32]{1,0:T(1,128)}, f32[1,32,512]{2,1,0:T(8,128)S(1)}, f32[4,1,32]{2,1,0:T(1,128)}, /*index=5*/f32[4,...) while((s32[]{:T(128)}, f32[1,32]{1,0:T(1,128)}, f32[1,32]{1,0:T(1,128)}, ...), condition=%wide.region_4.5_spmd, body=%wide.region_3.4_spmd.sunk | while | flops 49381 | bytes 198675 | solution.py:33
  55.2 0.7 fusion.80
  55.8 1.3 %fusion.81 = (f32[32]{0:T(128)S(1)}, f32[1,32]{1,0:T(1,128)}) fusion(f32[1,32]{1,0:T(1,128)S(1)} %get-tuple-element.313, f32[4,1,32]{2,1,0:T(1,128)} %get-tuple-element.316, s32[]{:T(128)S(6)} %select_n.70, f32[4,1,32]{2,1,0:T(1,128)} %get-tuple-element.317, f32[1,32]{1,0:T(1,128)} %get-tuple-element.304, f32[1,32]{1,0:T(1,128)} %get-tuple-element.303), kind=kLoop, calls=%fused_computation.13.clone.1 | loop fusion | flops 160 | bytes 900 | tf_op jit(solution)/shard_map/while/body/eval_jaxpr/exp | solution.py:56
  57.1 0.5 copy.103
  57.7 0.7 fusion.80
  58.4 1.3 %fusion.81 = (f32[32]{0:T(128)S(1)}, f32[1,32]{1,0:T(1,128)}) fusion(f32[1,32]{1,0:T(1,128)S(1)} %get-tuple-element.313, f32[4,1,32]{2,1,0:T(1,128)} %get-tuple-element.316, s32[]{:T(128)S(6)} %select_n.70, f32[4,1,32]{2,1,0:T(1,128)} %get-tuple-element.317, f32[1,32]{1,0:T(1,128)} %get-tuple-element.304, f32[1,32]{1,0:T(1,128)} %get-tuple-element.303), kind=kLoop, calls=%fused_computation.13.clone.1 | loop fusion | flops 160 | bytes 900 | tf_op jit(solution)/shard_map/while/body/eval_jaxpr/exp | solution.py:56
  59.6 0.5 copy.103
  60.2 0.7 fusion.80
  60.9 1.3 %fusion.81 = (f32[32]{0:T(128)S(1)}, f32[1,32]{1,0:T(1,128)}) fusion(f32[1,32]{1,0:T(1,128)S(1)} %get-tuple-element.313, f32[4,1,32]{2,1,0:T(1,128)} %get-tuple-element.316, s32[]{:T(128)S(6)} %select_n.70, f32[4,1,32]{2,1,0:T(1,128)} %get-tuple-element.317, f32[1,32]{1,0:T(1,128)} %get-tuple-element.304, f32[1,32]{1,0:T(1,128)} %get-tuple-element.303), kind=kLoop, calls=%fused_computation.13.clone.1 | loop fusion | flops 160 | bytes 900 | tf_op jit(solution)/shard_map/while/body/eval_jaxpr/exp | solution.py:56
  62.2 0.5 copy.103
  62.8 0.5 multiply_power_fusion
  63.3 1.3 %reshape.359 = bf16[8,64]{1,0:T(8,128)(2,1)} reshape(bf16[512]{0:T(512)(128)(2,1)} %copy-done.7) | data formatting | bytes 2048 | tf_op jit(solution)/shard_map/reshape.46
  64.7 3.7 %collective-permute-start.5 = (bf16[1,10,1024]{2,1,0:T(8,128)(2,1)S(1)}, bf16[1,10,1024]{2,1,0:T(8,128)(2,1)S(1)}, u32[]{:S(2)}, u32[]{:S(2)}) collective-permute-start(bf16[1,10,1024]{2,1,0:T(8,128)(2,1)S(1)} %copy.51), channel_id=1, source_target_pairs={{0,24},{4,28},{8,16},{12,20},{16,8},{20,12},{24,0},{28,4},{1,25},{... | collective-permute-start | bytes 61448 | tf_op jit(solution)/shard_map/ppermute | solution.py:79
  68.4 1.4 %bitcast_dynamic-update-slice_fusion.6 = bf16[8,1,10,1024]{3,2,1,0:T(8,128)(2,1)} fusion(bf16[8,1,10,1024]{3,2,1,0:T(8,128)(2,1)} %fusion.35, bf16[1,10,1024]{2,1,0:T(8,128)(2,1)} %collective-permute-done), kind=kLoop, calls=%fused_computation.57 | loop fusion | bytes 65536
  69.8 0.2 collective-permute-start.6
  70.0 1.4 %bitcast_dynamic-update-slice_fusion.5 = bf16[8,1,10,1024]{3,2,1,0:T(8,128)(2,1)} fusion(bf16[8,1,10,1024]{3,2,1,0:T(8,128)(2,1)} %bitcast_dynamic-update-slice_fusion.6, bf16[1,10,1024]{2,1,0:T(8,128)(2,1)} %collective-permute-done.1), kind=kLoop, calls=%fused_computation.56 | loop fusion | bytes 65536
  71.3 1.4 %bitcast_dynamic-update-slice_fusion.4 = bf16[8,1,10,1024]{3,2,1,0:T(8,128)(2,1)} fusion(bf16[8,1,10,1024]{3,2,1,0:T(8,128)(2,1)} %bitcast_dynamic-update-slice_fusion.5, bf16[1,10,1024]{2,1,0:T(8,128)(2,1)} %collective-permute-done.2), kind=kLoop, calls=%fused_computation.55 | loop fusion | bytes 65536
  72.7 1.4 %bitcast_dynamic-update-slice_fusion.3 = bf16[8,1,10,1024]{3,2,1,0:T(8,128)(2,1)} fusion(bf16[8,1,10,1024]{3,2,1,0:T(8,128)(2,1)} %bitcast_dynamic-update-slice_fusion.4, bf16[1,10,1024]{2,1,0:T(8,128)(2,1)} %collective-permute-done.3), kind=kLoop, calls=%fused_computation.54 | loop fusion | bytes 65536
  74.1 1.4 %bitcast_dynamic-update-slice_fusion.2 = bf16[8,1,10,1024]{3,2,1,0:T(8,128)(2,1)} fusion(bf16[8,1,10,1024]{3,2,1,0:T(8,128)(2,1)} %bitcast_dynamic-update-slice_fusion.3, bf16[1,10,1024]{2,1,0:T(8,128)(2,1)} %collective-permute-done.4), kind=kLoop, calls=%fused_computation.53 | loop fusion | bytes 65536
  75.5 0.6 bitcast_dynamic-update-slice_fusion.1
  76.1 0.3 collective-permute-done.6
  76.4 0.6 bitcast_dynamic-update-slice_fusion
  77.0 1.6 %gather_fusion = bf16[8,10,1024]{2,1,0:T(8,128)(2,1)S(1)} fusion(bf16[8,10,1024]{2,1,0:T(8,128)(2,1)} %bitcast.182, s32[1024]{0:T(1024)} %pad_clamp_fusion), kind=kCustom, calls=%fused_computation | custom fusion | bytes 327712 | tf_op jit(solution)/shard_map/gather | solution.py:80
  78.6 0.7 reshape_transpose.3
  79.4 7.4 %all_gather.27 = bf16[1,80,4096]{2,1,0:T(8,128)(2,1)S(1)} all-gather(bf16[1,80,1024]{2,1,0:T(8,128)(2,1)} %reshape_transpose.3), channel_id=1, replica_groups=mesh['sp'=8,'tp'=4] {'tp'}, dimensions={2}, use_global_device_ids=true | all-gather | bytes 819200 | tf_op jit(solution)/shard_map/all_gather | solution.py:87
  86.8 1.4 %convolution_bitcast_fusion = f32[1,80,64]{1,2,0:T(8,128)S(1)} fusion(bf16[4096,64]{0,1:T(8,128)(2,1)} %param.14, bf16[1,80,4096]{2,1,0:T(8,128)(2,1)S(1)} %all_gather.27), kind=kOutput, calls=%fused_computation.22 | convolution fusion | flops 41943040 | bytes 1200128 | tf_op jit(solution)/shard_map/dot_general | solution.py:91
  88.2 3.1 %multiply_reduce_fusion = (f32[80]{0:T(128)S(1)}, f32[80,512]{1,0:T(8,128)S(1)}) fusion(bf16[4096,512]{1,0:T(8,128)(2,1)} %param.13, bf16[1,80,4096]{2,1,0:T(8,128)(2,1)S(1)} %all_gather.27), kind=kOutput, calls=%fused_computation.47 | convolution fusion | flops 335626176 | bytes 5013824 | tf_op jit(solution)/shard_map/dot_general | solution.py:90
  91.3 0.4 convolution_convert_fusion.1
  91.7 0.4 convolution_convert_fusion
  92.5 0.6 pad_maximum_fusion
  93.1 0.2 fusion.65
  93.4 0.2 fusion.55
  93.7 0.3 fusion.15
  94.2 0.6 copy.84
  (58 shorter events, 1.3 us)
Async XLA Ops:
  0.6 34.4 %copy-start = (bf16[1,8192,64]{1,2,0:T(8,128)(2,1)S(1)}, bf16[1,8192,64]{1,2,0:T(8,128)(2,1)}, u32[]{:S(2)}) copy-start(bf16[1,8192,64]{1,2,0:T(8,128)(2,1)} %param.19) | copy-start | bytes 3145732
  3.6 61.2 %collective-permute-start = (bf16[1,10,1024]{2,1,0:T(8,128)(2,1)}, bf16[1,10,1024]{2,1,0:T(8,128)(2,1)}, u32[]{:S(2)}, u32[]{:S(2)}) collective-permute-start(bf16[1,10,1024]{2,1,0:T(8,128)(2,1)} %copy.46), channel_id=1, source_target_pairs={{0,4},{4,0},{8,12},{12,8},{16,20},{20,16},{24,28},{28,24},{1,5},{5... | collective-permute-start | bytes 61448 | tf_op jit(solution)/shard_map/ppermute | solution.py:79
  7.1 62.6 %collective-permute-start.1 = (bf16[1,10,1024]{2,1,0:T(8,128)(2,1)}, bf16[1,10,1024]{2,1,0:T(8,128)(2,1)}, u32[]{:S(2)}, u32[]{:S(2)}) collective-permute-start(bf16[1,10,1024]{2,1,0:T(8,128)(2,1)} %copy.47), channel_id=1, source_target_pairs={{0,8},{4,12},{8,0},{12,4},{16,24},{20,28},{24,16},{28,20},{1,9},{5... | collective-permute-start | bytes 61448 | tf_op jit(solution)/shard_map/ppermute | solution.py:79
  9.3 62.0 %collective-permute-start.2 = (bf16[1,10,1024]{2,1,0:T(8,128)(2,1)}, bf16[1,10,1024]{2,1,0:T(8,128)(2,1)}, u32[]{:S(2)}, u32[]{:S(2)}) collective-permute-start(bf16[1,10,1024]{2,1,0:T(8,128)(2,1)} %copy.48), channel_id=1, source_target_pairs={{0,12},{4,8},{8,4},{12,0},{16,28},{20,24},{24,20},{28,16},{1,13},{... | collective-permute-start | bytes 61448 | tf_op jit(solution)/shard_map/ppermute | solution.py:79
  10.0 62.7 %collective-permute-start.3 = (bf16[1,10,1024]{2,1,0:T(8,128)(2,1)}, bf16[1,10,1024]{2,1,0:T(8,128)(2,1)}, u32[]{:S(2)}, u32[]{:S(2)}) collective-permute-start(bf16[1,10,1024]{2,1,0:T(8,128)(2,1)} %copy.49), channel_id=1, source_target_pairs={{0,16},{4,20},{8,24},{12,28},{16,0},{20,4},{24,8},{28,12},{1,17},{... | collective-permute-start | bytes 61448 | tf_op jit(solution)/shard_map/ppermute | solution.py:79
  13.6 60.5 %collective-permute-start.4 = (bf16[1,10,1024]{2,1,0:T(8,128)(2,1)}, bf16[1,10,1024]{2,1,0:T(8,128)(2,1)}, u32[]{:S(2)}, u32[]{:S(2)}) collective-permute-start(bf16[1,10,1024]{2,1,0:T(8,128)(2,1)} %copy.50), channel_id=1, source_target_pairs={{0,20},{4,16},{8,28},{12,24},{16,4},{20,0},{24,12},{28,8},{1,21},{... | collective-permute-start | bytes 61448 | tf_op jit(solution)/shard_map/ppermute | solution.py:79
  16.1 0.6 copy-start.7
  22.0 13.8 %slice-start = ((s8[8388608]{0:T(1024)(128)(4,1)}), s8[4194304]{0:T(1024)(128)(4,1)S(1)}, s32[]{:S(2)}) async-start(s8[8388608]{0:T(1024)(128)(4,1)} %bitcast.179), calls=%async_computation | async-start | bytes 8388608
  28.9 6.8 %slice-start.1 = ((s8[8388608]{0:T(1024)(128)(4,1)}), s8[4194304]{0:T(1024)(128)(4,1)S(1)}, s32[]{:S(2)}) async-start(s8[8388608]{0:T(1024)(128)(4,1)} %bitcast.179), calls=%async_computation.1 | async-start | bytes 8388608
  35.8 1.7 %copy-start.13 = (u32[32]{0:T(128)S(1)}, u32[32]{0:T(128)}, u32[]{:S(2)}) copy-start(u32[32]{0:T(128)} %constant.107) | copy-start | bytes 388
  37.4 53.9 %copy-start.1 = (bf16[512,1024]{1,0:T(8,128)(2,1)S(1)}, bf16[512,1024]{1,0:T(8,128)(2,1)}, u32[]{:S(2)}) copy-start(bf16[512,1024]{1,0:T(8,128)(2,1)} %param.16) | copy-start | bytes 3145732
  37.4 54.3 %copy-start.2 = (bf16[512,1024]{1,0:T(8,128)(2,1)S(1)}, bf16[512,1024]{1,0:T(8,128)(2,1)}, u32[]{:S(2)}) copy-start(bf16[512,1024]{1,0:T(8,128)(2,1)} %param.17) | copy-start | bytes 3145732
  64.6 26.7 %copy-start.8 = (f32[512]{0:T(512)S(1)}, f32[512]{0:T(512)}, u32[]{:S(2)}) copy-start(f32[512]{0:T(512)} %param.15) | copy-start | bytes 6148
  64.6 27.4 %copy-start.12 = (bf16[1,1024]{1,0:T(2,128)(2,1)S(1)}, bf16[1,1024]{1,0:T(2,128)(2,1)}, u32[]{:S(2)}) copy-start(bf16[1,1024]{1,0:T(2,128)(2,1)} %param.20) | copy-start | bytes 6148
  64.6 27.6 %copy-start.10 = (f32[80]{0:T(128)S(1)}, f32[80]{0:T(128)}, u32[]{:S(2)}) copy-start(f32[80]{0:T(128)} %add_convert_fusion) | copy-start | bytes 964
  64.7 27.6 %copy-start.11 = (f32[32]{0:T(128)S(1)}, f32[32]{0:T(128)}, u32[]{:S(2)}) copy-start(f32[32]{0:T(128)} %multiply_power_fusion) | copy-start | bytes 388
  64.7 28.4 %copy-start.9 = (bf16[8,64]{1,0:T(8,128)(2,1)S(1)}, bf16[8,64]{1,0:T(8,128)(2,1)}, u32[]{:S(2)}) copy-start(bf16[8,64]{1,0:T(8,128)(2,1)} %reshape.359) | copy-start | bytes 3076
  64.7 28.6 %copy-start.5 = (f32[1,32]{1,0:T(1,128)S(1)}, f32[1,32]{1,0:T(1,128)}, u32[]{:S(2)}) copy-start(f32[1,32]{1,0:T(1,128)} %get-tuple-element.183) | copy-start | bytes 388
  64.7 28.9 %copy-start.6 = (f32[1,32]{1,0:T(1,128)S(1)}, f32[1,32]{1,0:T(1,128)}, u32[]{:S(2)}) copy-start(f32[1,32]{1,0:T(1,128)} %get-tuple-element.184) | copy-start | bytes 388
  64.7 10.7 %collective-permute-start.5 = (bf16[1,10,1024]{2,1,0:T(8,128)(2,1)S(1)}, bf16[1,10,1024]{2,1,0:T(8,128)(2,1)S(1)}, u32[]{:S(2)}, u32[]{:S(2)}) collective-permute-start(bf16[1,10,1024]{2,1,0:T(8,128)(2,1)S(1)} %copy.51), channel_id=1, source_target_pairs={{0,24},{4,28},{8,16},{12,20},{16,8},{20,12},{24,0},{28,4},{1,25},{... | collective-permute-start | bytes 61448 | tf_op jit(solution)/shard_map/ppermute | solution.py:79
  69.8 6.6 %collective-permute-start.6 = (bf16[1,10,1024]{2,1,0:T(8,128)(2,1)S(1)}, bf16[1,10,1024]{2,1,0:T(8,128)(2,1)S(1)}, u32[]{:S(2)}, u32[]{:S(2)}) collective-permute-start(bf16[1,10,1024]{2,1,0:T(8,128)(2,1)S(1)} %copy.52), channel_id=1, source_target_pairs={{0,28},{4,24},{8,20},{12,16},{16,12},{20,8},{24,4},{28,0},{1,29},{... | collective-permute-start | bytes 61448 | tf_op jit(solution)/shard_map/ppermute | solution.py:79
  91.7 3.2 %copy-start.3 = (bf16[80,1024]{1,0:T(8,128)(2,1)}, bf16[80,1024]{1,0:T(8,128)(2,1)S(1)}, u32[]{:S(2)}) copy-start(bf16[80,1024]{1,0:T(8,128)(2,1)S(1)} %convolution_convert_fusion.1) | copy-start | bytes 491524
  92.1 2.8 %copy-start.4 = (bf16[80,1024]{1,0:T(8,128)(2,1)}, bf16[80,1024]{1,0:T(8,128)(2,1)S(1)}, u32[]{:S(2)}) copy-start(bf16[80,1024]{1,0:T(8,128)(2,1)S(1)} %convolution_convert_fusion) | copy-start | bytes 491524
